TPU v7x, 256 devices: a whole 4x4x8 slice. The times are simulated.
256 devices in a mesh: sp: 64 (over z, y, core), tp: 4 (over x).
Axes of the slice: x: 4, y: 4, z: 8, core: 2. Of those that a mesh axis runs over, the one named last changes fastest.
Arguments:
- head_queries: bfloat16 [16384, 2048], P('sp', 'tp'), may hold values from -6 to 6
- head_keys: bfloat16 [16384, 2048], P('sp', 'tp'), may hold values from -6 to 6
- head_values: bfloat16 [16384, 2048], P('sp', 'tp'), may hold values from -6 to 6
- decay_logits: bfloat16 [16384, 2048], P('sp', 'tp'), may hold values from -12 to 1
- learning_logits: bfloat16 [16384, 32], P('sp', 'tp'), may hold values from -9 to 2
- surge_decay: float32 [16384, 32], P('sp', 'tp'), may hold values from -0.7 to 0
- documents: int32 [16384], P('sp'), may hold values from 0 to 16, never falling along the last dimension, each value on 1 to 1536 neighbouring positions
- residual: bfloat16 [16384, 2048], P(('sp', 'tp')), may hold values from -6 to 6
- head_norm_scale: float32 [2048], P('tp'), may hold values from 0.1 to 1.9
- mixer_output_weight: bfloat16 [2048, 2048], P('tp'), may hold values from -0.125 to 0.125
- layer_norm_scale: float32 [2048], replicated, may hold values from 0.1 to 1.9
- routes: int32 [16384, 2], P('sp'), may hold values from 0 to 127, all different within a row; in each aligned block of 64 rows (0 to 63, 64 to 127, ...) at most 2 rows name the same one
- routing_weight: float32 [16384, 2], P(('sp', 'tp')), may hold values from 0.3 to 1.5
- routed_gate_weight: bfloat16 [128, 2048, 1024], P('sp', None, 'tp'), may hold values from -0.125 to 0.125
- routed_up_weight: bfloat16 [128, 2048, 1024], P('sp', None, 'tp'), may hold values from -0.125 to 0.125
- routed_down_weight: bfloat16 [128, 1024, 2048], P('sp', 'tp'), may hold values from -0.1875 to 0.1875
- common_gate_weight: bfloat16 [2048, 512], P(None, 'tp'), may hold values from -0.125 to 0.125
- common_up_weight: bfloat16 [2048, 512], P(None, 'tp'), may hold values from -0.125 to 0.125
- common_down_weight: bfloat16 [512, 2048], P('tp'), may hold values from -0.25 to 0.25
Outputs:
- layer_out: bfloat16 [16384, 2048], P(('sp', 'tp'))
Inputs may be any that keep to these rules, and one draw needn't show every extreme that they name: `documents`: numbers never fall along the positions; each document holds 1 to 1536 positions and one holds exactly 1536. `routes`: each row names 2 different experts; in each aligned block of 64 rows no expert is named by more than 2 rows, a bound that some block reaches.
All inputs are finite; a program needn't handle non-finite values.
Results may differ from a plain program's by a relative error of at most 0.019.
Values may be sent and summed in bfloat16 or wider, within the bound.
A program may use at most 128 MiB of HBM per device.

v0:
```python
import jax
import jax.numpy as jnp
from jax import lax
from jax.sharding import Mesh
from jax.sharding import PartitionSpec as P

HEAD = 64
EXP_DEV = 2
TOP = 2
BLOCK_SPAN = 64
TOK_DEV = 64
SP = ("sp_0", "sp_1", "sp_2")
SP_TP = ("sp_0", "sp_1", "sp_2", "tp")
residual_scale = 2.0**0.5
group_eps = 0.00064
norm_eps = 1e-05
unit_eps = 1e-06
highest = lax.Precision.HIGHEST


def filled_with(x, identity):
    return jax.tree.map(
        lambda a, e: jnp.broadcast_to(jnp.asarray(e, a.dtype), a.shape), x, identity
    )


def all_in_one(x, axis):
    leaves = jax.tree.leaves(x)
    order = sorted(range(len(leaves)), key=lambda k: -leaves[k].size)
    width = (1, *leaves[order[0]].shape)[-1]
    lines = [
        jnp.pad(leaves[k].reshape(-1), (0, -leaves[k].size % width)).reshape(-1, width)
        for k in order
    ]
    both, at, found = (lax.all_gather(jnp.concatenate(lines), axis), 0, {})
    for k, line in zip(order, lines):
        piece = both[:, at : at + len(line)].reshape(len(both), -1)
        found[k] = piece[:, : leaves[k].size].reshape(-1, *leaves[k].shape)
        at += len(line)
    numbers = iter(range(len(leaves)))
    return jax.tree.map(lambda _: found[next(numbers)], x)


def prefix_by_axis(x, axes, combine, identity):
    before = start = filled_with(x, identity)
    running = x
    for axis in reversed(axes):
        devices, position = (lax.axis_size(axis), lax.axis_index(axis))
        pieces = all_in_one(
            jax.tree.map(
                lambda part, kind: part.astype(kind),
                running,
                (jnp.bfloat16, jnp.bfloat16, jnp.bfloat16, jnp.bfloat16),
            ),
            axis,
        )
        inside, running = (start, start)
        for k in range(devices):
            passed = k < position
            running = combine(
                running, jax.tree.map(lambda part, own: part[k].astype(own.dtype), pieces, x)
            )
            inside = jax.tree.map(lambda new, old: jnp.where(passed, new, old), running, inside)
        before = combine(inside, before)
    return before


def split_up(x, dim, devices):
    shape = x.shape
    pieces = x.reshape(*shape[:dim], devices, shape[dim] // devices, *shape[dim + 1 :])
    return jnp.moveaxis(pieces, dim, 0)


def sent_and_summed(x, axis, dim):
    pieces = split_up(x, dim, lax.axis_size(axis))
    arrived = lax.all_to_all(pieces, axis, split_axis=0, concat_axis=0, tiled=True)
    return arrived.astype(jnp.float32).sum(axis=0)


def pair_scores(left, right):
    return jnp.einsum("bhtn,bhsn->bhts", left, right, precision=highest)


def apply_scores(scores, operand):
    return jnp.einsum("bhts,bhsn->bhtn", scores, operand, precision=highest)


def split_heads(values, block_list, head_number):
    return (
        values.astype(jnp.float32)
        .reshape(block_list, BLOCK_SPAN, head_number, HEAD)
        .transpose(0, 2, 1, 3)
    )


def unit_lower_inverse(strict_part):
    power = strict_part
    inverse = jnp.eye(BLOCK_SPAN, dtype=jnp.float32) - strict_part
    reach = 2
    while reach < BLOCK_SPAN:
        power = apply_scores(power, power)
        inverse = inverse + apply_scores(inverse, power)
        reach = reach * 2
    return inverse


def link_states(earlier, later):
    map_one, add_one, first_one, last_one = earlier
    map_two, add_two, first_two, last_two = later
    joined = ((last_one == first_two) | (last_one < 0) | (first_two < 0)).astype(jnp.float32)
    map_out = joined * jnp.einsum("hij,hjk->hik", map_one, map_two, precision=highest)
    add_out = joined * jnp.einsum("hij,hjk->hik", add_one, map_two, precision=highest) + add_two
    first_out = jnp.where(first_one < 0, first_two, first_one)
    last_out = jnp.where(last_two < 0, last_one, last_two)
    return (map_out, add_out, first_out, last_out)


def linear_recurrence_mixer(
    head_queries,
    head_keys,
    head_values,
    decay_logits,
    learning_logits,
    surge_decay,
    documents,
    head_norm_scale,
):
    length, local_width = head_queries.shape
    head_number = local_width // HEAD
    block_list = length // BLOCK_SPAN
    read_heads = split_heads(head_queries, block_list, head_number)
    key_heads = split_heads(head_keys, block_list, head_number)
    values = split_heads(head_values, block_list, head_number)
    unit_keys = key_heads * lax.rsqrt(jnp.sum(key_heads * key_heads, -1, keepdims=True) + unit_eps)
    learn_rate = (
        jax.nn.sigmoid(learning_logits.astype(jnp.float32))
        .reshape(block_list, BLOCK_SPAN, head_number)
        .transpose(0, 2, 1)
    )
    surge_list = surge_decay.reshape(block_list, BLOCK_SPAN, head_number).transpose(0, 2, 1)
    decay_logarithm = split_heads(
        -jnp.exp(-jax.nn.softplus(-decay_logits.astype(jnp.float32)) - 0.5), block_list, head_number
    )
    decay_logarithm = decay_logarithm + surge_list[..., None]
    cumulative = jnp.cumsum(decay_logarithm, axis=2)
    before = cumulative - decay_logarithm
    doc_blocks = documents.reshape(block_list, BLOCK_SPAN)
    prior_doc = jnp.concatenate([doc_blocks[:1, 0], doc_blocks[:-1, -1]])
    joined = (doc_blocks == prior_doc[:, None]).astype(jnp.float32)[:, None, :, None]
    same_doc = doc_blocks[:, :, None] == doc_blocks[:, None, :]
    later_pos = lax.broadcasted_iota(jnp.int32, (BLOCK_SPAN, BLOCK_SPAN), 0)
    earlier_pos = lax.broadcasted_iota(jnp.int32, (BLOCK_SPAN, BLOCK_SPAN), 1)
    strict = (same_doc & (later_pos > earlier_pos)[None]).astype(jnp.float32)[:, None]
    causal_incl = (same_doc & (later_pos >= earlier_pos)[None]).astype(jnp.float32)[:, None]
    ahead_unit = unit_keys * jnp.exp(before)
    back_unit = unit_keys * jnp.exp(-cumulative)
    back_key = key_heads * jnp.exp(-cumulative)
    forward = read_heads * jnp.exp(cumulative)
    lower_part = pair_scores(ahead_unit, back_unit) * strict * learn_rate[:, :, None, :]
    mix_key = pair_scores(ahead_unit, back_key) * strict
    right_side = jnp.concatenate([ahead_unit * joined, apply_scores(mix_key, values)], -1)
    solved = apply_scores(unit_lower_inverse(lower_part), right_side)
    carry_map = solved[..., :HEAD]
    local_pull = solved[..., HEAD:]
    read_unit = pair_scores(forward, back_unit) * causal_incl * -learn_rate[:, :, None, :]
    read_key = pair_scores(forward, back_key) * causal_incl
    local_out = apply_scores(read_unit, local_pull) + apply_scores(read_key, values)
    read_start = forward * joined + apply_scores(read_unit, carry_map)
    block_total = cumulative[:, :, -1:, :]
    tail_mask = (doc_blocks == doc_blocks[:, -1:]).astype(jnp.float32)[:, None, :, None]
    end_unit = unit_keys * jnp.exp(block_total - cumulative) * tail_mask * -learn_rate[..., None]
    end_key = key_heads * jnp.exp(block_total - cumulative) * tail_mask
    block_map = jnp.eye(HEAD, dtype=jnp.float32) * (jnp.exp(block_total) * joined[:, :, -1:, :])
    block_map = block_map + jnp.einsum("bhsn,bhsm->bhnm", carry_map, end_unit, precision=highest)
    block_add = jnp.einsum("bhsv,bhsm->bhvm", local_pull, end_unit, precision=highest)
    block_add = block_add + jnp.einsum("bhsv,bhsm->bhvm", values, end_key, precision=highest)
    identity_map = jnp.broadcast_to(jnp.eye(HEAD, dtype=jnp.float32), (head_number, HEAD, HEAD))
    carried = jnp.zeros((head_number, HEAD, HEAD), jnp.float32)
    through = identity_map
    outputs = []
    starts = []
    for block_index in range(block_list):
        outputs.append(
            local_out[block_index]
            + jnp.einsum("hlm,hvm->hlv", read_start[block_index], carried, precision=highest)
        )
        starts.append(
            jnp.einsum("hlm,hnm->hln", read_start[block_index], through, precision=highest)
        )
        carried = (
            jnp.einsum("hvn,hnm->hvm", carried, block_map[block_index], precision=highest)
            + block_add[block_index]
        )
        through = jnp.einsum("hvn,hnm->hvm", through, block_map[block_index], precision=highest)
    first_doc = documents[0].astype(jnp.float32)
    last_doc = documents[-1].astype(jnp.float32)
    no_doc = jnp.full((), -1.0, jnp.float32)
    identity = (identity_map, jnp.zeros((head_number, HEAD, HEAD), jnp.float32), no_doc, no_doc)
    prefix = prefix_by_axis((through, carried, first_doc, last_doc), SP, link_states, identity)
    incoming = prefix[1] * (prefix[3] == first_doc).astype(jnp.float32)
    head_read = jnp.stack(outputs) + jnp.einsum(
        "bhln,hvn->bhlv", jnp.stack(starts), incoming, precision=highest
    )
    centre = jnp.mean(head_read, -1, keepdims=True)
    spread = jnp.mean(jnp.square(head_read - centre), -1, keepdims=True)
    normed = (
        ((head_read - centre) * lax.rsqrt(spread + group_eps))
        .transpose(0, 2, 1, 3)
        .reshape(length, local_width)
    )
    return (normed * head_norm_scale).astype(jnp.bfloat16)


def per_device(
    head_queries,
    head_keys,
    head_values,
    decay_logits,
    learning_logits,
    surge_decay,
    documents,
    residual,
    head_norm_scale,
    mixer_output_weight,
    layer_norm_scale,
    routes,
    routing_weight,
    routed_gate_weight,
    routed_up_weight,
    routed_down_weight,
    common_gate_weight,
    common_up_weight,
    common_down_weight,
):
    head_outputs = linear_recurrence_mixer(
        head_queries,
        head_keys,
        head_values,
        decay_logits,
        learning_logits,
        surge_decay,
        documents,
        head_norm_scale,
    )
    mixed_rows = sent_and_summed(
        jnp.dot(head_outputs, mixer_output_weight, preferred_element_type=jnp.float32).astype(
            jnp.bfloat16
        ),
        "tp",
        0,
    )
    summed = residual_scale * residual.astype(jnp.float32) + mixed_rows
    centre = jnp.mean(summed, -1, keepdims=True)
    spread = jnp.mean(jnp.square(summed - centre), -1, keepdims=True)
    stream = ((summed - centre) * lax.rsqrt(spread + norm_eps) * layer_norm_scale).astype(
        jnp.bfloat16
    )
    quarters = lax.axis_size("tp")
    groups = lax.axis_size(SP)
    experts = EXP_DEV * groups
    capacity = max(2, (3 * TOK_DEV * TOP + 2 * experts - 1) // (2 * experts))
    own_rows, model_width = stream.shape
    chosen = routes.reshape(quarters, own_rows * TOP)
    onehot = (chosen[..., None] == jnp.arange(experts, dtype=jnp.int32)).astype(jnp.int32)
    ranking = jnp.sum(jnp.cumsum(onehot, 1) * onehot, -1) - 1
    slot_index = chosen * capacity + ranking
    own_slots = lax.dynamic_index_in_dim(slot_index, lax.axis_index("tp"), 0, keepdims=False)
    outgoing = jnp.zeros((experts * capacity, model_width), jnp.bfloat16)
    outgoing = outgoing.at[own_slots].set(jnp.repeat(stream, TOP, axis=0))
    arrived = lax.all_to_all(
        outgoing.reshape(groups, EXP_DEV, capacity, model_width),
        SP,
        split_axis=0,
        concat_axis=0,
        tiled=True,
    )
    arrived_all, rows_all = (
        lax.all_gather(arrived[None], "tp", axis=0, tiled=True),
        lax.all_gather(stream, "tp", axis=0, tiled=True),
    )
    gated = jnp.einsum(
        "qsecd,edf->qsecf", arrived_all, routed_gate_weight, preferred_element_type=jnp.float32
    )
    lifted = jnp.einsum(
        "qsecd,edf->qsecf", arrived_all, routed_up_weight, preferred_element_type=jnp.float32
    )
    hidden = (jax.nn.silu(gated) * lifted).astype(jnp.bfloat16)
    partial_value = jnp.einsum(
        "qsecf,efd->qsecd", hidden, routed_down_weight, preferred_element_type=jnp.float32
    )
    shared_gated = jnp.dot(rows_all, common_gate_weight, preferred_element_type=jnp.float32)
    shared_lifted = jnp.dot(rows_all, common_up_weight, preferred_element_type=jnp.float32)
    shared_hidden = (jax.nn.silu(shared_gated) * shared_lifted).astype(jnp.bfloat16)
    shared_part = jnp.dot(shared_hidden, common_down_weight, preferred_element_type=jnp.float32)
    expert_sum, shared_sum = (
        sent_and_summed(partial_value.astype(jnp.bfloat16), "tp", 0),
        sent_and_summed(shared_part.astype(jnp.bfloat16), "tp", 0),
    )
    returned = lax.all_to_all(
        expert_sum[0].astype(jnp.bfloat16), SP, split_axis=0, concat_axis=0, tiled=True
    )
    picked = returned.reshape(experts * capacity, model_width)[own_slots]
    weighted = (
        picked.astype(jnp.float32).reshape(own_rows, TOP, model_width) * routing_weight[:, :, None]
    )
    routed = jnp.sum(weighted, 1)
    return (residual_scale * stream.astype(jnp.float32) + routed + shared_sum).astype(jnp.bfloat16)


def solution(mesh):
    torus = Mesh(mesh.devices.reshape(8, 4, 2, mesh.shape["tp"]), ("sp_0", "sp_1", "sp_2", "tp"))
    placed = (
        P(SP, "tp"),
        P(SP, "tp"),
        P(SP, "tp"),
        P(SP, "tp"),
        P(SP, "tp"),
        P(SP, "tp"),
        P(SP),
        P(SP_TP, None),
        P("tp"),
        P("tp", None),
        P(),
        P(SP, None),
        P(SP_TP, None),
        P(SP, None, "tp"),
        P(SP, None, "tp"),
        P(SP, "tp", None),
        P(None, "tp"),
        P(None, "tp"),
        P("tp", None),
    )
    return jax.shard_map(
        per_device, mesh=torus, in_specs=placed, out_specs=P(SP_TP, None), check_vma=False
    )
```

profile of v0, /device:TPU:1, one launch (start us, length us, event | category | flops | bytes accessed | tf_op | source)
XLA Modules:
  0.0 536.4 jit_solution(10089789795744124520)
XLA Ops:
  14.4 2.3 reshape.498
  22.5 3.1 convolution_multiply_fusion.1
  25.6 2.2 fusion.17
  35.1 12.9 %convolution_add_fusion.2 = f32[4,8,64,64]{3,2,1,0:T(8,128)S(1)} fusion(f32[4,8,64,64]{3,2,1,0:T(8,128)S(1)} %convolution_add_fusion.3, f32[4,8,64,64]{3,2,1,0:T(8,128)S(1)} %fusion.188), kind=kOutput, calls=%fused_computation.17 | convolution fusion | flops 100794368 | bytes 1572864 | tf_op jit(solution)/shard_map/bhts,bhsn->bhtn/dot_general | solution.py:85
  48.0 2.2 fusion.190
  50.2 2.2 convolution_add_fusion.1
  53.8 3.2 convolution_add_fusion
  60.7 3.0 convolution_add_fusion.5
  63.7 2.5 convolution_add_fusion.6
  72.0 2.1 convolution_convert_fusion.2
  81.6 5.0 all-gather.4
  102.9 2.0 convolution_add_fusion.12
  107.4 2.1 fusion.182
  110.5 2.0 fusion.181
  115.7 10.6 %all-gather.5 = bf16[4,1026,64]{1,2,0:T(8,128)(2,1)S(1)} all-gather(bf16[1,1026,64]{1,2,0:T(8,128)(2,1)} %bitcast.420), channel_id=3, replica_groups=mesh['sp_0'=8,'sp_1'=4,'sp_2'=2,'tp'=4] {'sp_1'}, dimensions={0}, use_global_device_ids=true | all-gather | bytes 656640 | tf_op jit(solution)/shard_map/all_gather | solution.py:35
  149.5 2.0 convolution_add_fusion.11
  164.7 2.1 fusion.184
  171.6 1.9 fusion.183
  176.8 2.2 reshape.578
  178.9 4.2 fusion.18
  183.2 3.4 convolution_multiply_fusion
  186.5 3.1 fusion.80
  196.6 2.3 convolution_bitcast_fusion.2
  198.9 2.6 convolution_add_fusion.8
  209.4 5.8 %all-gather.15.cloned.1.call-done = bf16[8,1026,64]{1,2,0:T(8,128)(2,1)} async-done(((bf16[1,1026,64]{1,2,0:T(8,128)(2,1)}), bf16[8,1026,64]{1,2,0:T(8,128)(2,1)}) %all-gather.15.cloned.1.call-update) | async-done | bytes 1050640 | tf_op jit(solution)/shard_map/all_gather | solution.py:35
  237.1 2.1 fusion.172
  259.4 3.1 fusion.185
  266.1 3.3 convolution_convert_fusion.1
  269.4 4.3 all-to-all-start
  274.8 1.9 reduce_window_sum.23
  278.0 5.5 %all-to-all-done = bf16[4,64,2048]{2,1,0:T(8,128)(2,1)S(1)} async-done(((bf16[4,64,2048]{2,1,0:T(8,128)(2,1)}), bf16[4,64,2048]{2,1,0:T(8,128)(2,1)S(1)}, u32[]{:S(2)}, u32[]{:S(2)}) %all-to-all-start) | async-done | bytes 1048608 | tf_op jit(solution)/shard_map/all_to_all | solution.py:76
  285.9 2.2 scatter_custom_fusion
  289.6 42.3 %all_to_all.25 = bf16[64,2,2,2048]{3,2,1,0:T(2,128)(2,1)} all-to-all(bf16[64,2,2,2048]{3,2,1,0:T(2,128)(2,1)} %reshape.531), channel_id=1, replica_groups=mesh['sp_0'=8,'sp_1'=4,'sp_2'=2,'tp'=4] {'sp_0','sp_1','sp_2'}, dimensions={0} | all-to-all | bytes 2097152 | tf_op jit(solution)/shard_map/all_to_all | solution.py:270
  331.9 45.8 %all-gather.13.cloned.1.call-done = bf16[256,2,2,2048]{3,2,1,0:T(2,128)(2,1)} async-done(((bf16[64,2,2,2048]{3,2,1,0:T(2,128)(2,1)}), bf16[256,2,2,2048]{3,2,1,0:T(2,128)(2,1)}) %all-gather.13.cloned.1.call-update) | async-done | bytes 4194320 | tf_op jit(solution)/shard_map/all_gather | solution.py:278
  377.7 4.6 copy.284
  382.3 2.0 copy-done.17
  385.6 7.3 %convert_bitcast_fusion = bf16[4,1,64,2,2,2048]{5,2,4,0,3,1:T(8,128)(2,1)} fusion(bf16[2,256,2048]{2,1,0:T(8,128)(2,1)S(1)} %copy-done, bf16[2,2048,256]{2,1,0:T(8,128)(2,1)} %param.33, bf16[4,64,2,2,2048]{4,1,0,3,2:T(8,128)(2,1)} %bitcast.391, f32[4,64,2,2,256]{4,1,3,0,2:T(8,128)S(1)} %fusion.7), kind=kOutput, calls=%fused_computation.2 | convolution fusion | flops 2151153664 | bytes 13631488 | tf_op jit(solution)/shard_map/qsecf,efd->qsecd/dot_general | solution.py:288
  392.9 4.8 copy.287
  397.7 4.9 all-to-all-start.2
  403.3 36.8 %all-gather.11.cloned.1.call-done = bf16[256,2048]{1,0:T(8,128)(2,1)} async-done(((bf16[64,2048]{1,0:T(8,128)(2,1)}), bf16[256,2048]{1,0:T(8,128)(2,1)}) %all-gather.11.cloned.1.call-update) | async-done | bytes 1048592 | tf_op jit(solution)/shard_map/all_gather | solution.py:279
  441.9 2.9 convolution_convert_fusion
  444.9 14.2 %all-to-all-done.2 = bf16[4,1,64,2,2,2048]{5,2,4,3,1,0:T(8,128)(2,1)} async-done(((bf16[4,1,64,2,2,2048]{5,2,4,3,1,0:T(8,128)(2,1)}), bf16[4,1,64,2,2,2048]{5,2,4,3,1,0:T(8,128)(2,1)}, u32[]{:S(2)}, u32[]{:S(2)}) %all-to-all-start.2) | async-done | bytes 4194336 | tf_op jit(solution)/shard_map/all_to_all | solution.py:76
  459.1 7.8 %all-to-all-start.4 = ((bf16[4,64,2048]{2,1,0:T(8,128)(2,1)}), bf16[4,64,2048]{2,1,0:T(8,128)(2,1)S(1)}, u32[]{:S(2)}, u32[]{:S(2)}) async-start(bf16[4,64,2048]{2,1,0:T(8,128)(2,1)} %bitcast.137), calls=%async_computation.4 | async-start | bytes 2097152 | tf_op jit(solution)/shard_map/all_to_all | solution.py:76
  466.9 4.3 reduce_sum.100
  471.2 3.3 copy.289
  474.5 6.7 %all-to-all-done.4 = bf16[4,64,2048]{2,1,0:T(8,128)(2,1)S(1)} async-done(((bf16[4,64,2048]{2,1,0:T(8,128)(2,1)}), bf16[4,64,2048]{2,1,0:T(8,128)(2,1)S(1)}, u32[]{:S(2)}, u32[]{:S(2)}) %all-to-all-start.4) | async-done | bytes 1048608 | tf_op jit(solution)/shard_map/all_to_all | solution.py:76
  481.2 11.9 %all-to-all-start.3 = ((bf16[64,2,2,2048]{3,2,1,0:T(2,128)(2,1)}), bf16[64,2,2,2048]{3,2,1,0:T(2,128)(2,1)}, u32[]{:S(2)}, u32[]{:S(2)}) async-start(bf16[64,2,2,2048]{3,2,1,0:T(2,128)(2,1)} %copy.289), calls=%async_computation.3 | async-start | bytes 2097152 | tf_op jit(solution)/shard_map/all_to_all | solution.py:299
  494.2 27.0 %all-to-all-done.3 = bf16[64,2,2,2048]{3,2,1,0:T(2,128)(2,1)} async-done(((bf16[64,2,2,2048]{3,2,1,0:T(2,128)(2,1)}), bf16[64,2,2,2048]{3,2,1,0:T(2,128)(2,1)}, u32[]{:S(2)}, u32[]{:S(2)}) %all-to-all-start.3) | async-done | bytes 1048608 | tf_op jit(solution)/shard_map/all_to_all | solution.py:299
  (324 shorter events, 145.6 us)
Async XLA Ops:
  6.5 379.0 %copy-start = (bf16[2,256,2048]{2,1,0:T(8,128)(2,1)S(1)}, bf16[2,256,2048]{2,1,0:T(8,128)(2,1)}, u32[]{:S(2)}) copy-start(bf16[2,256,2048]{2,1,0:T(8,128)(2,1)} %param.34) | copy-start | bytes 6291460
  6.5 6.6 %copy-start.71 = (bf16[256,8]{0,1:T(8,128)(2,1)S(1)}, bf16[256,8]{0,1:T(8,128)(2,1)}, u32[]{:S(2)}) copy-start(bf16[256,8]{0,1:T(8,128)(2,1)} %param.23) | copy-start | bytes 12292
  6.5 6.7 %copy-start.57 = (bf16[256,512]{1,0:T(8,128)(2,1)S(1)}, bf16[256,512]{1,0:T(8,128)(2,1)}, u32[]{:S(2)}) copy-start(bf16[256,512]{1,0:T(8,128)(2,1)} %param.22) | copy-start | bytes 786436
  6.5 208.6 %all-gather.15.cloned.1.call-start = ((), (), s32[]{:S(2)}) async-start(), calls=%async_computation.7 | async-start | bytes 1327104 | tf_op jit(solution)/shard_map/all_gather | solution.py:35
  12.7 4.1 copy-start.1
  12.7 4.0 copy-start.70
  16.8 3.8 copy-start.10
  53.5 3.5 copy-start.12
  53.5 3.5 copy-start.19
  66.2 3.8 copy-start.11
  66.5 3.4 copy-start.21
  178.9 4.2 copy-start.4
  178.9 4.2 copy-start.7
  178.9 4.2 copy-start.43
  183.2 3.4 copy-start.6
  191.3 5.3 copy-start.20
  191.3 7.6 %copy-start.13 = (bf16[4,64,8,64]{3,2,1,0:T(8,128)(2,1)S(1)}, bf16[4,64,8,64]{3,2,1,0:T(8,128)(2,1)}, u32[]{:S(2)}) copy-start(bf16[4,64,8,64]{3,2,1,0:T(8,128)(2,1)} %reshape.502) | copy-start | bytes 786436
  196.6 5.0 copy-start.9
  198.9 4.0 copy-start.31
  198.9 5.2 copy-start.41
  201.5 3.9 copy-start.29
  201.6 5.1 copy-start.42
  201.6 5.1 copy-start.47
  202.9 4.2 copy-start.24
  202.9 4.2 copy-start.27
  202.9 4.2 copy-start.34
  202.9 4.2 copy-start.49
  204.1 4.1 copy-start.32
  204.1 4.1 copy-start.36
  204.1 4.1 copy-start.39
  204.1 4.1 copy-start.50
  252.9 3.8 copy-start.53
  252.9 4.1 copy-start.54
  252.9 4.3 copy-start.55
  254.2 3.3 copy-start.44
  254.2 3.3 copy-start.56
  266.0 7.7 %copy-start.73 = (s32[256,2]{0,1:T(2,128)S(1)}, s32[256,2]{0,1:T(2,128)}, u32[]{:S(2)}) copy-start(s32[256,2]{0,1:T(2,128)} %param.30) | copy-start | bytes 6148
  269.4 14.2 %copy-start.25 = (bf16[64,2048]{1,0:T(8,128)(2,1)S(1)}, bf16[64,2048]{1,0:T(8,128)(2,1)}, u32[]{:S(2)}) copy-start(bf16[64,2048]{1,0:T(8,128)(2,1)} %param.26) | copy-start | bytes 786436
  269.4 14.1 %all-to-all-start = ((bf16[4,64,2048]{2,1,0:T(8,128)(2,1)}), bf16[4,64,2048]{2,1,0:T(8,128)(2,1)S(1)}, u32[]{:S(2)}, u32[]{:S(2)}) async-start(bf16[4,64,2048]{2,1,0:T(8,128)(2,1)} %bitcast.123), calls=%async_computation | async-start | bytes 2097152 | tf_op jit(solution)/shard_map/all_to_all | solution.py:76
  273.7 104.0 %all-gather.13.cloned.1.call-start = ((), (), s32[]{:S(2)}) async-start(), calls=%async_computation.6 | async-start | bytes 5242880 | tf_op jit(solution)/shard_map/all_gather | solution.py:278
  274.0 10.0 %copy-start.69 = (f32[2048]{0:T(1024)S(1)}, f32[2048]{0:T(1024)}, u32[]{:S(2)}) copy-start(f32[2048]{0:T(1024)} %param.29) | copy-start | bytes 24580
  284.5 5.1 copy-start.15
  377.7 6.6 %copy-start.77 = (bf16[2,2048,256]{2,1,0:T(8,128)(2,1)S(1)}, bf16[2,2048,256]{2,1,0:T(8,128)(2,1)}, u32[]{:S(2)}) copy-start(bf16[2,2048,256]{2,1,0:T(8,128)(2,1)} %param.32) | copy-start | bytes 6291460
  397.7 61.4 %all-to-all-start.2 = ((bf16[4,1,64,2,2,2048]{5,2,4,3,1,0:T(8,128)(2,1)}), bf16[4,1,64,2,2,2048]{5,2,4,3,1,0:T(8,128)(2,1)}, u32[]{:S(2)}, u32[]{:S(2)}) async-start(bf16[4,1,64,2,2,2048]{5,2,4,3,1,0:T(8,128)(2,1)} %copy.287), calls=%async_computation.2 | async-start | bytes 8388608 | tf_op jit(solution)/shard_map/all_to_all | solution.py:76
  402.6 37.5 %all-gather.11.cloned.1.call-start = ((), (), s32[]{:S(2)}) async-start(), calls=%async_computation.5 | async-start | bytes 1310720 | tf_op jit(solution)/shard_map/all_gather | solution.py:279
  459.1 22.1 %all-to-all-start.4 = ((bf16[4,64,2048]{2,1,0:T(8,128)(2,1)}), bf16[4,64,2048]{2,1,0:T(8,128)(2,1)S(1)}, u32[]{:S(2)}, u32[]{:S(2)}) async-start(bf16[4,64,2048]{2,1,0:T(8,128)(2,1)} %bitcast.137), calls=%async_computation.4 | async-start | bytes 2097152 | tf_op jit(solution)/shard_map/all_to_all | solution.py:76
  471.2 22.0 %copy-start.75 = (f32[64,2]{0,1:T(2,128)S(1)}, f32[64,2]{0,1:T(2,128)}, u32[]{:S(2)}) copy-start(f32[64,2]{0,1:T(2,128)} %param.31) | copy-start | bytes 1540
  481.2 40.0 %all-to-all-start.3 = ((bf16[64,2,2,2048]{3,2,1,0:T(2,128)(2,1)}), bf16[64,2,2,2048]{3,2,1,0:T(2,128)(2,1)}, u32[]{:S(2)}, u32[]{:S(2)}) async-start(bf16[64,2,2,2048]{3,2,1,0:T(2,128)(2,1)} %copy.289), calls=%async_computation.3 | async-start | bytes 2097152 | tf_op jit(solution)/shard_map/all_to_all | solution.py:299
  (37 other events, 65.5 us)
Sparse Core Ops, SparseCore 0:
  176.9 38.2 all-gather.14
  332.0 45.6 all-gather.12
  405.2 34.8 all-gather.10
where the time goes:
time: 542 us; the launch traced here: 536 us
  waiting for transfers between devices  142 us (26%)
  matrix products  123 us (23%)
  local copies, waits for them, and re-layouts  104 us (19%)
  blocking collectives  58 us (11%)
  between operations  55 us (10%)
  starting transfers between devices  29.2 us (5%)
  other arithmetic  25.1 us (5%)
    all_gather x1, waiting for transfers between devices, per_device(): lax.all_gather(arrived[None], 'tp', axis=0, tiled=True)  45.8 us
    all_to_all x1, blocking collectives, per_device(): lax.all_to_all(outgoing.reshape(groups, EXP_DEV, capacity, model_width),...  42.3 us
    dot_general x15, matrix products, apply_scores(): return jnp.einsum('bhts,bhsn->bhtn', scores, operand, precision=highest)  37 us
    all_gather x1, waiting for transfers between devices, per_device(): lax.all_gather(stream, 'tp', axis=0, tiled=True)  36.8 us
    all_to_all x1, waiting for transfers between devices, per_device(): lax.all_to_all(expert_sum[0].astype(jnp.bfloat16), SP, split_axis=0, conc...  27 us
    all_to_all x3, waiting for transfers between devices, sent_and_summed(): lax.all_to_all(pieces, axis, split_axis=0, concat_axis=0, tiled=True)  26.4 us
    dot_general x17, matrix products, link_states(): jnp.einsum('hij,hjk->hik', add_one, map_two, precision=highest)  17.7 us
    reshape x18, local copies, waits for them, and re-layouts, all_in_one(): jnp.pad(leaves[k].reshape(-1), (0, -leaves[k].size % width))  17.2 us
  transfers between devices with their start and end apart: 7, of which 7 were waited for; matrix products, arithmetic and copies ran while one was open for 9% of the time, Pallas kernels for 0%

commit v1 on v0

--- a/solution.py
+++ b/solution.py
@@ -16,6 +16,28 @@
 norm_eps = 1e-05
 unit_eps = 1e-06
 highest = lax.Precision.HIGHEST
+
+
+def in_order(blocks, dim):
+    blocks = jnp.moveaxis(blocks, 0, dim)
+    dims = blocks.shape
+    return blocks.reshape(*dims[:dim], dims[dim] * dims[dim + 1], *dims[dim + 2 :])
+
+
+def gather_around(value, axis, dim):
+    size = lax.axis_size(axis)
+    pairs = [(i, (i + 1) % size) for i in range(size)]
+    back = [(b, a) for a, b in pairs]
+    lower, upper = ([], [])
+    for step in range(size - 1):
+        if step % 2 == 0:
+            lower.append(lax.ppermute(lower[-1] if lower else value, axis, pairs))
+        else:
+            upper.append(lax.ppermute(upper[-1] if upper else value, axis, back))
+    parts = jnp.stack([*lower[::-1], value, *upper])
+    shift = lax.axis_index(axis) - len(lower)
+    parts = parts[(jnp.arange(size) - shift) % size]
+    return in_order(parts, dim)
 
 
 def filled_with(x, identity):
@@ -276,7 +298,7 @@
     )
     arrived_all, rows_all = (
         lax.all_gather(arrived[None], "tp", axis=0, tiled=True),
-        lax.all_gather(stream, "tp", axis=0, tiled=True),
+        gather_around(stream, "tp", 0),
     )
     gated = jnp.einsum(
         "qsecd,edf->qsecf", arrived_all, routed_gate_weight, preferred_element_type=jnp.float32

time: 542 us -> 537 us (level)
  matrix products: 123 us -> 111 us
    ppermute x0 -> x3, waiting for transfers between devices: none -> 57.7 us  [the longest x2 57.7 us: gather_around(): lower.append(lax.ppermute(lower[-1] if lower else value, axis, pairs))]
    all_gather x1 -> x0, waiting for transfers between devices: 36.8 us -> none  [per_device(): lax.all_gather(stream, 'tp', axis=0, tiled=True)]
    all_to_all x3, waiting for transfers between devices: 26.4 us -> 10.2 us  [sent_and_summed(): lax.all_to_all(pieces, axis, split_axis=0, concat_axis=0, tiled=True)]
    dot_general x15, matrix products: 37 us -> 25.8 us  [apply_scores(): return jnp.einsum('bhts,bhsn->bhtn', scores, operand, precision=highest)]
  transfers between devices with their start and end apart: 7 -> 9, of which waited for: 7 -> 7; matrix products, arithmetic and copies ran while one was open for 9% -> 10% of each run, Pallas kernels for 0% -> 0%
where the time goes in v1:
time: 537 us; the launch traced here: 531 us
  waiting for transfers between devices  146 us (27%)
  matrix products  111 us (21%)
  local copies, waits for them, and re-layouts  106 us (20%)
  blocking collectives  58 us (11%)
  between operations  54 us (10%)
  starting transfers between devices  29.4 us (5%)
  other arithmetic  26 us (5%)
    ppermute x2, waiting for transfers between devices, gather_around(): lower.append(lax.ppermute(lower[-1] if lower else value, axis, pairs))  57.7 us
    all_gather x1, waiting for transfers between devices, per_device(): lax.all_gather(arrived[None], 'tp', axis=0, tiled=True)  45.8 us
    all_to_all x1, blocking collectives, per_device(): lax.all_to_all(outgoing.reshape(groups, EXP_DEV, capacity, model_width),...  42.5 us
    all_to_all x1, waiting for transfers between devices, per_device(): lax.all_to_all(expert_sum[0].astype(jnp.bfloat16), SP, split_axis=0, conc...  27 us
    dot_general x15, matrix products, apply_scores(): return jnp.einsum('bhts,bhsn->bhtn', scores, operand, precision=highest)  25.8 us
    dot_general x17, matrix products, link_states(): jnp.einsum('hij,hjk->hik', add_one, map_two, precision=highest)  17.8 us
    reshape x18, local copies, waits for them, and re-layouts, all_in_one(): jnp.pad(leaves[k].reshape(-1), (0, -leaves[k].size % width))  17.4 us
    convert_element_type x14, local copies, waits for them, and re-layouts, prefix_by_axis(): part[k].astype(own.dtype)  16.3 us
  transfers between devices with their start and end apart: 9, of which 7 were waited for; matrix products, arithmetic and copies ran while one was open for 10% of the time, Pallas kernels for 0%

profile of v1, /device:TPU:1, one launch (start us, length us, event | category | flops | bytes accessed | tf_op | source)
XLA Modules:
  0.0 531.0 jit_solution(15452122540909762920)
XLA Ops:
  14.5 2.3 reshape.550
  22.5 3.1 convolution_multiply_fusion.1
  25.6 2.2 fusion.17
  36.7 2.2 fusion.192
  39.0 2.2 convolution_add_fusion.1
  42.5 3.2 convolution_add_fusion
  49.4 3.0 convolution_add_fusion.5
  52.4 2.5 convolution_add_fusion.6
  60.7 2.1 convolution_convert_fusion.2
  70.5 5.0 all-gather.4
  91.5 2.0 convolution_add_fusion.12
  96.0 2.1 fusion.184
  99.1 2.0 fusion.183
  104.3 10.4 %all-gather.5 = bf16[4,1026,64]{1,2,0:T(8,128)(2,1)S(1)} all-gather(bf16[1,1026,64]{1,2,0:T(8,128)(2,1)} %bitcast.431), channel_id=3, replica_groups=mesh['sp_0'=8,'sp_1'=4,'sp_2'=2,'tp'=4] {'sp_1'}, dimensions={0}, use_global_device_ids=true | all-gather | bytes 656640 | tf_op jit(solution)/shard_map/all_gather | solution.py:57
  135.0 1.9 fusion.131
  136.9 2.0 convolution_add_fusion.11
  152.1 2.0 fusion.186
  159.0 1.9 fusion.185
  164.1 2.1 reshape.631
  166.3 4.2 fusion.18
  170.5 3.4 convolution_multiply_fusion
  173.9 3.1 fusion.80
  184.1 2.3 convolution_bitcast_fusion.2
  186.4 2.6 convolution_add_fusion.8
  196.9 5.6 %all-gather.12.cloned.1.call-done = bf16[8,1026,64]{1,2,0:T(8,128)(2,1)} async-done(((bf16[1,1026,64]{1,2,0:T(8,128)(2,1)}), bf16[8,1026,64]{1,2,0:T(8,128)(2,1)}) %all-gather.12.cloned.1.call-update) | async-done | bytes 1050640 | tf_op jit(solution)/shard_map/all_gather | solution.py:57
  224.3 2.2 fusion.174
  246.6 3.1 fusion.187
  253.2 3.3 convolution_convert_fusion.1
  256.5 4.1 all-to-all-start
  261.8 1.9 reduce_window_sum.23
  264.9 5.5 %all-to-all-done = bf16[4,64,2048]{2,1,0:T(8,128)(2,1)S(1)} async-done(((bf16[4,64,2048]{2,1,0:T(8,128)(2,1)}), bf16[4,64,2048]{2,1,0:T(8,128)(2,1)S(1)}, u32[]{:S(2)}, u32[]{:S(2)}) %all-to-all-start) | async-done | bytes 1048608 | tf_op jit(solution)/shard_map/all_to_all | solution.py:98
  272.8 2.2 scatter_custom_fusion
  276.5 42.5 %all_to_all.25 = bf16[64,2,2,2048]{3,2,1,0:T(2,128)(2,1)} all-to-all(bf16[64,2,2,2048]{3,2,1,0:T(2,128)(2,1)} %reshape.583), channel_id=1, replica_groups=mesh['sp_0'=8,'sp_1'=4,'sp_2'=2,'tp'=4] {'sp_0','sp_1','sp_2'}, dimensions={0} | all-to-all | bytes 2097152 | tf_op jit(solution)/shard_map/all_to_all | solution.py:292
  319.1 45.8 %all-gather.10.cloned.1.call-done = bf16[256,2,2,2048]{3,2,1,0:T(2,128)(2,1)} async-done(((bf16[64,2,2,2048]{3,2,1,0:T(2,128)(2,1)}), bf16[256,2,2,2048]{3,2,1,0:T(2,128)(2,1)}) %all-gather.10.cloned.1.call-update) | async-done | bytes 4194320 | tf_op jit(solution)/shard_map/all_gather | solution.py:300
  364.8 4.6 copy.284
  369.5 2.0 copy-done.14
  372.7 7.3 %convert_bitcast_fusion = bf16[4,1,64,2,2,2048]{5,2,4,0,3,1:T(8,128)(2,1)} fusion(bf16[2,256,2048]{2,1,0:T(8,128)(2,1)S(1)} %copy-done, bf16[2,2048,256]{2,1,0:T(8,128)(2,1)} %param.33, bf16[4,64,2,2,2048]{4,1,0,3,2:T(8,128)(2,1)} %bitcast.401, f32[4,64,2,2,256]{4,1,3,0,2:T(8,128)S(1)} %fusion.7), kind=kOutput, calls=%fused_computation.3 | convolution fusion | flops 2151153664 | bytes 13631488 | tf_op jit(solution)/shard_map/qsecf,efd->qsecd/dot_general | solution.py:310
  380.1 4.8 copy.287
  384.8 4.9 all-to-all-start.2
  392.7 50.4 %collective-permute-done = bf16[64,2048]{1,0:T(8,128)(2,1)S(1)} collective-permute-done((bf16[64,2048]{1,0:T(8,128)(2,1)S(1)}, bf16[64,2048]{1,0:T(8,128)(2,1)S(1)}, u32[]{:S(2)}, u32[]{:S(2)}) %collective-permute-start) | collective-permute-done | bytes 262176 | tf_op jit(solution)/shard_map/ppermute | solution.py:34
  443.1 7.3 %collective-permute-done.1 = bf16[64,2048]{1,0:T(8,128)(2,1)S(1)} collective-permute-done((bf16[64,2048]{1,0:T(8,128)(2,1)S(1)}, bf16[64,2048]{1,0:T(8,128)(2,1)S(1)}, u32[]{:S(2)}, u32[]{:S(2)}) %collective-permute-start.1) | collective-permute-done | bytes 262176 | tf_op jit(solution)/shard_map/ppermute | solution.py:34
  454.9 2.9 convolution_convert_fusion
  457.8 3.5 all-to-all-start.4
  461.3 4.3 reduce_sum.100
  465.6 3.3 copy.289
  469.0 4.7 all-to-all-done.4
  473.6 13.9 %all-to-all-start.3 = ((bf16[64,2,2,2048]{3,2,1,0:T(2,128)(2,1)}), bf16[64,2,2,2048]{3,2,1,0:T(2,128)(2,1)}, u32[]{:S(2)}, u32[]{:S(2)}) async-start(bf16[64,2,2,2048]{3,2,1,0:T(2,128)(2,1)} %copy.289), calls=%async_computation.3 | async-start | bytes 2097152 | tf_op jit(solution)/shard_map/all_to_all | solution.py:321
  488.6 27.0 %all-to-all-done.3 = bf16[64,2,2,2048]{3,2,1,0:T(2,128)(2,1)} async-done(((bf16[64,2,2,2048]{3,2,1,0:T(2,128)(2,1)}), bf16[64,2,2,2048]{3,2,1,0:T(2,128)(2,1)}, u32[]{:S(2)}, u32[]{:S(2)}) %all-to-all-start.3) | async-done | bytes 1048608 | tf_op jit(solution)/shard_map/all_to_all | solution.py:321
  (325 shorter events, 150.1 us)
Async XLA Ops:
  6.5 366.2 %copy-start = (bf16[2,256,2048]{2,1,0:T(8,128)(2,1)S(1)}, bf16[2,256,2048]{2,1,0:T(8,128)(2,1)}, u32[]{:S(2)}) copy-start(bf16[2,256,2048]{2,1,0:T(8,128)(2,1)} %param.34) | copy-start | bytes 6291460
  6.5 6.6 %copy-start.68 = (bf16[256,8]{0,1:T(8,128)(2,1)S(1)}, bf16[256,8]{0,1:T(8,128)(2,1)}, u32[]{:S(2)}) copy-start(bf16[256,8]{0,1:T(8,128)(2,1)} %param.23) | copy-start | bytes 12292
  6.5 6.8 %copy-start.54 = (bf16[256,512]{1,0:T(8,128)(2,1)S(1)}, bf16[256,512]{1,0:T(8,128)(2,1)}, u32[]{:S(2)}) copy-start(bf16[256,512]{1,0:T(8,128)(2,1)} %param.22) | copy-start | bytes 786436
  6.5 196.0 %all-gather.12.cloned.1.call-start = ((), (), s32[]{:S(2)}) async-start(), calls=%async_computation.6 | async-start | bytes 1327104 | tf_op jit(solution)/shard_map/all_gather | solution.py:57
  12.8 4.1 copy-start.1
  12.8 4.0 copy-start.67
  16.9 3.9 copy-start.10
  42.2 3.5 copy-start.12
  42.2 3.5 copy-start.16
  54.9 3.8 copy-start.11
  55.2 3.4 copy-start.18
  166.3 4.2 copy-start.4
  166.3 4.2 copy-start.7
  166.3 4.2 copy-start.40
  170.5 3.4 copy-start.6
  178.6 5.4 %copy-start.17 = (f32[8,64,64]{2,1,0:T(8,128)S(1)}, f32[8,64,64]{2,1,0:T(8,128)}, u32[]{:S(2)}) copy-start(f32[8,64,64]{2,1,0:T(8,128)} %fusion.118) | copy-start | bytes 393220
  178.6 7.8 %copy-start.13 = (bf16[4,64,8,64]{3,2,1,0:T(8,128)(2,1)S(1)}, bf16[4,64,8,64]{3,2,1,0:T(8,128)(2,1)}, u32[]{:S(2)}) copy-start(bf16[4,64,8,64]{3,2,1,0:T(8,128)(2,1)} %reshape.554) | copy-start | bytes 786436
  184.1 5.0 copy-start.9
  186.4 3.9 copy-start.28
  186.4 5.2 copy-start.38
  189.1 3.9 copy-start.26
  189.1 5.1 copy-start.39
  189.1 5.1 copy-start.44
  190.3 4.2 copy-start.21
  190.3 4.2 copy-start.24
  190.3 4.3 copy-start.31
  190.4 4.3 copy-start.46
  191.6 4.1 copy-start.29
  191.6 4.1 copy-start.33
  191.6 4.1 copy-start.36
  191.6 4.1 copy-start.47
  240.1 3.8 copy-start.50
  240.1 4.1 copy-start.51
  240.1 4.3 copy-start.52
  241.4 3.3 copy-start.41
  253.2 7.4 %copy-start.70 = (s32[256,2]{0,1:T(2,128)S(1)}, s32[256,2]{0,1:T(2,128)}, u32[]{:S(2)}) copy-start(s32[256,2]{0,1:T(2,128)} %param.30) | copy-start | bytes 6148
  256.5 14.0 %copy-start.22 = (bf16[64,2048]{1,0:T(8,128)(2,1)S(1)}, bf16[64,2048]{1,0:T(8,128)(2,1)}, u32[]{:S(2)}) copy-start(bf16[64,2048]{1,0:T(8,128)(2,1)} %param.26) | copy-start | bytes 786436
  256.5 13.8 %all-to-all-start = ((bf16[4,64,2048]{2,1,0:T(8,128)(2,1)}), bf16[4,64,2048]{2,1,0:T(8,128)(2,1)S(1)}, u32[]{:S(2)}, u32[]{:S(2)}) async-start(bf16[4,64,2048]{2,1,0:T(8,128)(2,1)} %bitcast.123), calls=%async_computation | async-start | bytes 2097152 | tf_op jit(solution)/shard_map/all_to_all | solution.py:98
  260.6 104.2 %all-gather.10.cloned.1.call-start = ((), (), s32[]{:S(2)}) async-start(), calls=%async_computation.5 | async-start | bytes 5242880 | tf_op jit(solution)/shard_map/all_gather | solution.py:300
  260.9 10.0 %copy-start.66 = (f32[2048]{0:T(1024)S(1)}, f32[2048]{0:T(1024)}, u32[]{:S(2)}) copy-start(f32[2048]{0:T(1024)} %param.29) | copy-start | bytes 24580
  364.8 6.6 %copy-start.74 = (bf16[2,2048,256]{2,1,0:T(8,128)(2,1)S(1)}, bf16[2,2048,256]{2,1,0:T(8,128)(2,1)}, u32[]{:S(2)}) copy-start(bf16[2,2048,256]{2,1,0:T(8,128)(2,1)} %param.32) | copy-start | bytes 6291460
  384.8 73.0 %all-to-all-start.2 = ((bf16[4,1,64,2,2,2048]{5,2,4,3,1,0:T(8,128)(2,1)}), bf16[4,1,64,2,2,2048]{5,2,4,3,1,0:T(8,128)(2,1)}, u32[]{:S(2)}, u32[]{:S(2)}) async-start(bf16[4,1,64,2,2,2048]{5,2,4,3,1,0:T(8,128)(2,1)} %copy.287), calls=%async_computation.2 | async-start | bytes 8388608 | tf_op jit(solution)/shard_map/all_to_all | solution.py:98
  389.7 53.3 %collective-permute-start = (bf16[64,2048]{1,0:T(8,128)(2,1)S(1)}, bf16[64,2048]{1,0:T(8,128)(2,1)S(1)}, u32[]{:S(2)}, u32[]{:S(2)}) collective-permute-start(bf16[64,2048]{1,0:T(8,128)(2,1)S(1)} %multiply_convert_fusion), channel_id=1, source_target_pairs={{0,1},{1,2},{2,3},{3,0},{4,5},{5,6},{6,7},{7,4},{8,9},{9,10},{10,1... | collective-permute-start | bytes 786440 | tf_op jit(solution)/shard_map/ppermute | solution.py:34
  391.3 51.8 %collective-permute-start.2 = (bf16[64,2048]{1,0:T(8,128)(2,1)S(1)}, bf16[64,2048]{1,0:T(8,128)(2,1)S(1)}, u32[]{:S(2)}, u32[]{:S(2)}) collective-permute-start(bf16[64,2048]{1,0:T(8,128)(2,1)S(1)} %multiply_convert_fusion), channel_id=1, source_target_pairs={{1,0},{2,1},{3,2},{0,3},{5,4},{6,5},{7,6},{4,7},{9,8},{10,9},{11,1... | collective-permute-start | bytes 786440 | tf_op jit(solution)/shard_map/ppermute | solution.py:36
  443.1 7.4 %collective-permute-start.1 = (bf16[64,2048]{1,0:T(8,128)(2,1)S(1)}, bf16[64,2048]{1,0:T(8,128)(2,1)S(1)}, u32[]{:S(2)}, u32[]{:S(2)}) collective-permute-start(bf16[64,2048]{1,0:T(8,128)(2,1)S(1)} %collective-permute-done), channel_id=1, source_target_pairs={{0,1},{1,2},{2,3},{3,0},{4,5},{5,6},{6,7},{7,4},{8,9},{9,10},{10,1... | collective-permute-start | bytes 786440 | tf_op jit(solution)/shard_map/ppermute | solution.py:34
  457.8 15.8 %all-to-all-start.4 = ((bf16[4,64,2048]{2,1,0:T(8,128)(2,1)}), bf16[4,64,2048]{2,1,0:T(8,128)(2,1)S(1)}, u32[]{:S(2)}, u32[]{:S(2)}) async-start(bf16[4,64,2048]{2,1,0:T(8,128)(2,1)} %bitcast.399), calls=%async_computation.4 | async-start | bytes 2097152 | tf_op jit(solution)/shard_map/all_to_all | solution.py:98
  465.6 21.9 %copy-start.72 = (f32[64,2]{0,1:T(2,128)S(1)}, f32[64,2]{0,1:T(2,128)}, u32[]{:S(2)}) copy-start(f32[64,2]{0,1:T(2,128)} %param.31) | copy-start | bytes 1540
  473.6 42.0 %all-to-all-start.3 = ((bf16[64,2,2,2048]{3,2,1,0:T(2,128)(2,1)}), bf16[64,2,2,2048]{3,2,1,0:T(2,128)(2,1)}, u32[]{:S(2)}, u32[]{:S(2)}) async-start(bf16[64,2,2,2048]{3,2,1,0:T(2,128)(2,1)} %copy.289), calls=%async_computation.3 | async-start | bytes 2097152 | tf_op jit(solution)/shard_map/all_to_all | solution.py:321
  (36 other events, 63.8 us)
Sparse Core Ops, SparseCore 0:
  164.3 38.2 all-gather.11
  319.2 45.6 all-gather.9
